TPU v7x, 32 devices: a whole 2x2x4 slice. The times are simulated.
32 devices in a mesh: grp: 2 (over x), kv: 4 (over z), tp: 4 (over y, core).
Axes of the slice: x: 2, y: 2, z: 4, core: 2. Of those that a mesh axis runs over, the one named last changes fastest.
Arguments:
- x_rows: bfloat16 [256, 4096], P('grp', 'kv'), parts along dimension 0, may hold values from -32 to 32
- in_gain: bfloat16 [4096], P('kv'), may hold values from 0.099609375 to 1.8984375
- query_weight: bfloat16 [4096, 4096], P('kv', 'tp'), may hold values from -0.09375 to 0.09375
- key_weight: bfloat16 [4096, 4096], P('kv', 'tp'), may hold values from -0.09375 to 0.09375
- value_weight: bfloat16 [4096, 8192], P('kv', 'tp'), may hold values from -0.09375 to 0.09375
- outgate_weight: bfloat16 [4096, 8192], P('kv', 'tp'), may hold values from -0.09375 to 0.09375
- input_gate_weight: bfloat16 [4096, 32], P('kv', 'tp'), may hold values from -0.09375 to 0.09375
- forget_gate_weight: bfloat16 [4096, 32], P('kv', 'tp'), may hold values from -0.09375 to 0.09375
- forget_bias: float32 [32], P('tp'), may hold values from -1 to 3
- state_matrix: float32 [256, 32, 128, 256], P(('grp', 'kv'), 'tp'), parts along dimension 0, may hold values from -3 to 3
- state_norm: float32 [256, 32, 128], P(('grp', 'kv'), 'tp'), parts along dimension 0, may hold values from -6 to 6
- state_max: float32 [256, 32], P(('grp', 'kv'), 'tp'), parts along dimension 0, may hold values from -1 to 1
- head_gain: bfloat16 [8192], P('tp'), may hold values from 0.099609375 to 1.8984375
- out_weight: bfloat16 [8192, 4096], P('tp', 'kv'), may hold values from -0.0625 to 0.0625
- mix_gain: bfloat16 [4096], P('kv'), may hold values from 0.099609375 to 1.8984375
- up_weight: bfloat16 [4096, 16384], P('kv', 'tp'), may hold values from -0.09375 to 0.09375
- down_weight: bfloat16 [16384, 4096], P('tp', 'kv'), may hold values from -0.046875 to 0.046875
Outputs:
- mixed_out: bfloat16 [256, 4096], P('grp', 'kv'), parts along dimension 0
- new_matrix: float32 [256, 32, 128, 256], P(('grp', 'kv'), 'tp'), parts along dimension 0
- new_norm: float32 [256, 32, 128], P(('grp', 'kv'), 'tp'), parts along dimension 0
- new_max: float32 [256, 32], P(('grp', 'kv'), 'tp'), parts along dimension 0
There are 2 independent parts, one for each index of `grp`. A program takes and returns all parts, laid end to end along the dimension named above; an argument that names none is the same for every part. Nothing has to cross between parts.
All inputs are finite; a program needn't handle non-finite values.
Results may differ from a plain program's by a relative error of at most 0.019.
Values may be sent and summed in bfloat16 or wider, within the bound.
A program may use at most 192 MiB of HBM per device.

v0:
```python
import jax
import jax.numpy as jnp
from jax import lax
from jax.sharding import PartitionSpec as P

D = 4096
DQK = 128
DV = 256
epsilon = 1e-06


def per_device(
    x_rows,
    in_gain,
    query_weight,
    key_weight,
    value_weight,
    outgate_weight,
    input_gate_weight,
    forget_gate_weight,
    forget_bias,
    state_matrix,
    state_norm,
    state_max,
    head_gain,
    out_weight,
    mix_gain,
    up_weight,
    down_weight,
):
    xfull = x_rows.astype(jnp.float32)
    partial_squares = jnp.sum(xfull * xfull, axis=1)
    scaled = (xfull * in_gain.astype(jnp.float32)).astype(jnp.bfloat16)
    gate_columns = jnp.concatenate([input_gate_weight, forget_gate_weight], axis=1)

    def product(weight):
        return jnp.dot(scaled, weight, preferred_element_type=jnp.float32)

    query_part, key_part, value_part, outgate_part, gate_part, squares = (
        lax.psum_scatter(product(query_weight), "kv", scatter_dimension=0, tiled=True),
        lax.psum_scatter(product(key_weight), "kv", scatter_dimension=0, tiled=True),
        lax.psum_scatter(product(value_weight), "kv", scatter_dimension=0, tiled=True),
        lax.psum_scatter(product(outgate_weight), "kv", scatter_dimension=0, tiled=True),
        lax.psum_scatter(product(gate_columns), "kv", scatter_dimension=0, tiled=True),
        lax.psum_scatter(partial_squares, "kv", scatter_dimension=0, tiled=True),
    )
    scale = lax.rsqrt(squares / D + epsilon)[:, None]
    row_count = state_max.shape[0]
    head_count = state_max.shape[1]

    def rounded(partial_value):
        return lax.optimization_barrier((partial_value * scale).astype(jnp.bfloat16)).astype(
            jnp.float32
        )

    query = rounded(query_part).reshape(row_count, head_count, DQK) * DQK ** (-0.5)
    keys = rounded(key_part).reshape(row_count, head_count, DQK)
    values = rounded(value_part).reshape(row_count, head_count, DV)
    outgate = rounded(outgate_part).reshape(row_count, head_count, DV)
    gates = gate_part * scale
    igate = gates[:, :head_count]
    fgate = gates[:, head_count:]
    log_forget = jax.nn.log_sigmoid(fgate + forget_bias[None, :])
    new_max = jnp.maximum(log_forget + state_max, igate)
    fdecay = jnp.exp(log_forget + state_max - new_max)
    idecay = jnp.exp(igate - new_max)
    new_matrix = fdecay[:, :, None, None] * state_matrix + idecay[:, :, None, None] * (
        keys[:, :, :, None] * values[:, :, None, :]
    )
    new_norm = fdecay[:, :, None] * state_norm + idecay[:, :, None] * keys
    numer = jnp.einsum("bhd,bhde->bhe", query, new_matrix, precision=lax.Precision.HIGHEST)
    denom = jnp.sum(query * new_norm, axis=-1)
    readout = numer / jnp.maximum(jnp.abs(denom), jnp.exp(-new_max))[:, :, None]
    normed = readout * lax.rsqrt(jnp.mean(readout * readout, axis=-1, keepdims=True) + epsilon)
    normed = normed * head_gain.astype(jnp.float32).reshape(head_count, DV)
    merged = (
        (jax.nn.sigmoid(outgate) * normed).reshape(row_count, head_count * DV).astype(jnp.bfloat16)
    )
    branch = jnp.dot(
        lax.all_gather(merged, "kv", axis=0, tiled=True),
        out_weight,
        preferred_element_type=jnp.float32,
    )
    branch = lax.psum(branch, "tp")
    resid = lax.optimization_barrier((xfull + branch).astype(jnp.bfloat16)).astype(jnp.float32)
    partial_two = jnp.sum(resid * resid, axis=1)
    scaled_two = (resid * mix_gain.astype(jnp.float32)).astype(jnp.bfloat16)
    up_part = jnp.dot(scaled_two, up_weight, preferred_element_type=jnp.float32)
    up_total, squares_two = (
        lax.psum_scatter(up_part, "kv", scatter_dimension=0, tiled=True),
        lax.psum_scatter(partial_two, "kv", scatter_dimension=0, tiled=True),
    )
    scale_two = lax.rsqrt(squares_two / D + epsilon)[:, None]
    hidden = jnp.square(jax.nn.relu(up_total * scale_two)).astype(jnp.bfloat16)
    down = jnp.dot(
        lax.all_gather(hidden, "kv", axis=0, tiled=True),
        down_weight,
        preferred_element_type=jnp.float32,
    )
    down = lax.psum(down.astype(jnp.bfloat16), "tp").astype(jnp.float32)
    mixed_out = (resid + down).astype(jnp.bfloat16)
    return (mixed_out, new_matrix, new_norm, new_max)


def solution(mesh):
    placed = (
        P("grp", "kv"),
        P("kv"),
        P("kv", "tp"),
        P("kv", "tp"),
        P("kv", "tp"),
        P("kv", "tp"),
        P("kv", "tp"),
        P("kv", "tp"),
        P("tp"),
        P(("grp", "kv"), "tp", None, None),
        P(("grp", "kv"), "tp", None),
        P(("grp", "kv"), "tp"),
        P("tp"),
        P("tp", "kv"),
        P("kv"),
        P("kv", "tp"),
        P("tp", "kv"),
    )
    return jax.shard_map(
        per_device,
        mesh=mesh,
        in_specs=placed,
        out_specs=(
            P("grp", "kv"),
            P(("grp", "kv"), "tp", None, None),
            P(("grp", "kv"), "tp", None),
            P(("grp", "kv"), "tp"),
        ),
        check_vma=False,
    )
```

profile of v0, /device:TPU:0, one launch (start us, length us, event | category | flops | bytes accessed | tf_op | source)
XLA Modules:
  0.0 355.6 jit_solution(17088462818694971066)
XLA Ops:
  7.2 0.8 convert_element_type.61
  8.1 1.8 fusion.14
  10.0 2.2 fusion.16
  12.3 3.0 fusion.12
  15.3 4.0 %fusion.10 = f32[128,2048]{1,0:T(8,128)} fusion(bf16[1024,2048]{1,0:T(8,128)(2,1)} %param.21, bf16[128,1024]{1,0:T(8,128)(2,1)} %param.17, f32[1024]{0:T(1024)S(1)} %convert_element_type.61), kind=kOutput, calls=%fused_computation.30 | convolution fusion | flops 537264128 | bytes 5509120 | tf_op jit(solution)/shard_map/dot_general | solution.py:37
  19.4 3.9 %fusion.18 = f32[128,2048]{1,0:T(8,128)} fusion(bf16[1024,2048]{1,0:T(8,128)(2,1)} %param.22, bf16[128,1024]{1,0:T(8,128)(2,1)S(1)} %copy-done.2, f32[1024]{0:T(1024)S(1)} %convert_element_type.61), kind=kOutput, calls=%fused_computation.34 | convolution fusion | flops 537264128 | bytes 5509120 | tf_op jit(solution)/shard_map/dot_general | solution.py:37
  23.5 0.6 dynamic-slice
  24.9 13.4 %all-reduce = f32[128]{0:T(128)S(1)} all-reduce(f32[128]{0:T(128)S(1)} %fusion.1), channel_id=3, replica_groups=mesh['grp'=2,'kv'=4,'tp'=4] {'kv'}, use_global_device_ids=true, to_apply=%region_2.0.clone | all-reduce | flops 128 | bytes 1024
  38.4 0.8 broadcast_multiply_fusion
  39.3 15.9 %reduce-scatter.11.cloned.1.call-done = f32[32,1024]{1,0:T(8,128)} async-done(((f32[128,1024]{1,0:T(8,128)}), f32[32,1024]{1,0:T(8,128)}) %reduce-scatter.11.cloned.1.call-update) | async-done | bytes 131088 | tf_op jit(solution)/shard_map/reduce_scatter | solution.py:40
  55.2 22.4 %reduce-scatter.13.cloned.1.call-done = f32[32,1024]{1,0:T(8,128)} async-done(((f32[128,1024]{1,0:T(8,128)}), f32[32,1024]{1,0:T(8,128)}) %reduce-scatter.13.cloned.1.call-update) | async-done | bytes 131088 | tf_op jit(solution)/shard_map/reduce_scatter | solution.py:41
  77.6 1.1 multiply_convert_fusion.3
  79.1 26.9 %reduce-scatter.15.cloned.1.call-done = f32[32,2048]{1,0:T(8,128)} async-done(((f32[128,2048]{1,0:T(8,128)}), f32[32,2048]{1,0:T(8,128)}) %reduce-scatter.15.cloned.1.call-update) | async-done | bytes 262160 | tf_op jit(solution)/shard_map/reduce_scatter | solution.py:42
  105.9 27.9 %reduce-scatter.9.cloned.1.call-done = f32[32,2048]{1,0:T(8,128)} async-done(((f32[128,2048]{1,0:T(8,128)}), f32[32,2048]{1,0:T(8,128)}) %reduce-scatter.9.cloned.1.call-update) | async-done | bytes 262160 | tf_op jit(solution)/shard_map/reduce_scatter | solution.py:43
  133.9 1.1 multiply_convert_fusion.1
  135.2 24.5 %multiply_add_fusion = f32[32,8,128,256]{3,2,1,0:T(8,128)} fusion(f32[32,8,128,256]{3,2,1,0:T(8,128)} %param.26, f32[32,8,256]{2,1,0:T(8,128)S(1)} %bitcast.45, f32[32,8,128]{2,1,0:T(8,128)S(1)} %bitcast.44, f32[32,8]{1,0:T(8,128)S(1)} %subtract_exponential_fusion, f32[32,8]{1,0:T(8,128)S(1)} %get-tuple-element.8), kind=kLoop, calls=%fused_computation | loop fusion | flops 33554432 | bytes 67504128 | tf_op jit(solution)/shard_map/add | solution.py:67
  159.8 19.8 %fusion.31 = f32[32,8,1,256]{3,2,1,0:T(1,128)S(1)} fusion(f32[32,8,128,1]{2,3,1,0:T(1,128)S(1)} %bitcast.43, f32[32,8,128,256]{3,2,1,0:T(8,128)} %multiply_add_fusion), kind=kOutput, calls=%fused_computation.56 | convolution fusion | flops 100663296 | bytes 33947648 | tf_op jit(solution)/shard_map/bhd,bhde->bhe/dot_general | solution.py:71
  179.6 0.2 multiply_reduce_fusion
  179.8 0.1 fusion.8
  179.9 16.0 %all_gather.6 = bf16[128,2048]{1,0:T(8,128)(2,1)S(1)} all-gather(bf16[32,2048]{1,0:T(8,128)(2,1)S(1)} %bitcast.47), channel_id=1, replica_groups=mesh['grp'=2,'kv'=4,'tp'=4] {'kv'}, dimensions={0}, use_global_device_ids=true | all-gather | bytes 655360 | tf_op jit(solution)/shard_map/all_gather | solution.py:80
  195.9 1.6 fusion.32
  197.5 31.9 %all-reduce.5.cloned.1.call-done = f32[128,1024]{1,0:T(8,128)} async-done(((f32[128,1024]{1,0:T(8,128)}), f32[128,1024]{1,0:T(8,128)}) %all-reduce.5.cloned.1.call-update) | async-done | bytes 524304 | tf_op jit(solution)/shard_map/psum | solution.py:84
  229.4 1.1 fusion.2
  230.5 6.0 %fusion.6 = f32[128,4096]{1,0:T(8,128)} fusion(bf16[1024,4096]{1,0:T(8,128)(2,1)} %param.32, bf16[128,1024]{1,0:T(8,128)(2,1)S(1)} %fusion.2, f32[1024]{0:T(1024)S(1)} %convert_element_type.73), kind=kOutput, calls=%fused_computation.15 | convolution fusion | flops 1074135040 | bytes 10752000 | tf_op jit(solution)/shard_map/dot_general | solution.py:88
  236.7 11.8 %all-reduce.1 = f32[128]{0:T(128)S(1)} all-reduce(f32[128]{0:T(128)S(1)} %fusion.4), channel_id=9, replica_groups=mesh['grp'=2,'kv'=4,'tp'=4] {'kv'}, use_global_device_ids=true, to_apply=%region_12.13.clone | all-reduce | flops 128 | bytes 1024
  248.6 31.8 %reduce-scatter.17.cloned.1.call-done = f32[32,4096]{1,0:T(8,128)} async-done(((f32[128,4096]{1,0:T(8,128)}), f32[32,4096]{1,0:T(8,128)}) %reduce-scatter.17.cloned.1.call-update) | async-done | bytes 524304 | tf_op jit(solution)/shard_map/reduce_scatter | solution.py:90
  280.5 1.9 multiply_convert_fusion
  282.4 27.4 %all-gather.2.cloned.1.call-done = bf16[128,4096]{1,0:T(8,128)(2,1)} async-done(((bf16[32,4096]{1,0:T(8,128)(2,1)}), bf16[128,4096]{1,0:T(8,128)(2,1)}) %all-gather.2.cloned.1.call-update) | async-done | bytes 1048592 | tf_op jit(solution)/shard_map/all_gather | solution.py:96
  309.8 5.7 %convolution_convert_fusion = bf16[128,1024]{1,0:T(8,128)(2,1)} fusion(bf16[128,4096]{1,0:T(8,128)(2,1)} %all-gather.2.cloned.1.call-done, bf16[4096,1024]{1,0:T(8,128)(2,1)} %param.33), kind=kOutput, calls=%fused_computation.1 | convolution fusion | flops 1073872896 | bytes 9699328 | tf_op jit(solution)/shard_map/dot_general | solution.py:95
  315.5 0.7 copy.28
  316.2 31.2 %all-reduce.7.cloned.1.call-done = bf16[128,1024]{1,0:T(8,128)(2,1)} async-done(((bf16[128,1024]{1,0:T(8,128)(2,1)}), bf16[128,1024]{1,0:T(8,128)(2,1)}) %all-reduce.7.cloned.1.call-update) | async-done | bytes 262160 | tf_op jit(solution)/shard_map/psum | solution.py:100
  347.3 1.7 fusion.5
  (62 shorter events, 1.8 us)
Async XLA Ops:
  7.2 2.8 copy-start
  7.2 12.2 %copy-start.2 = (bf16[128,1024]{1,0:T(8,128)(2,1)S(1)}, bf16[128,1024]{1,0:T(8,128)(2,1)}, u32[]{:S(2)}) copy-start(bf16[128,1024]{1,0:T(8,128)(2,1)} %param.17) | copy-start | bytes 786436
  7.2 31.2 %reduce-scatter.19.cloned.1.call-start = ((), (), s32[]{:S(2)}) async-start(), calls=%async_computation.14 | async-start | bytes 81920 | tf_op jit(solution)/shard_map/reduce_scatter | solution.py:44
  9.9 45.3 %reduce-scatter.11.cloned.1.call-start = ((), (), s32[]{:S(2)}) async-start(), calls=%async_computation.7 | async-start | bytes 655360 | tf_op jit(solution)/shard_map/reduce_scatter | solution.py:40
  12.2 11.3 %copy-start.10 = (u32[32]{0:T(128)S(1)}, u32[32]{0:T(128)}, u32[]{:S(2)}) copy-start(u32[32]{0:T(128)} %constant.23) | copy-start | bytes 388
  12.2 12.5 %copy-start.6 = (bf16[2048]{0:T(1024)(128)(2,1)S(1)}, bf16[2048]{0:T(1024)(128)(2,1)}, u32[]{:S(2)}) copy-start(bf16[2048]{0:T(1024)(128)(2,1)} %param.29) | copy-start | bytes 12292
  12.2 12.6 %copy-start.7 = (f32[32,8]{0,1:T(8,128)S(1)}, f32[32,8]{0,1:T(8,128)}, u32[]{:S(2)}) copy-start(f32[32,8]{0,1:T(8,128)} %param.28) | copy-start | bytes 3076
  12.2 26.9 %copy-start.9 = (f32[8]{0:T(128)S(1)}, f32[8]{0:T(128)}, u32[]{:S(2)}) copy-start(f32[8]{0:T(128)} %param.25) | copy-start | bytes 100
  12.3 65.4 %reduce-scatter.13.cloned.1.call-start = ((), (), s32[]{:S(2)}) async-start(), calls=%async_computation.8 | async-start | bytes 655360 | tf_op jit(solution)/shard_map/reduce_scatter | solution.py:41
  15.3 63.5 %copy-start.5 = (f32[32,8,128]{2,1,0:T(8,128)S(1)}, f32[32,8,128]{2,1,0:T(8,128)}, u32[]{:S(2)}) copy-start(f32[32,8,128]{2,1,0:T(8,128)} %param.27) | copy-start | bytes 393220
  15.3 90.7 %reduce-scatter.15.cloned.1.call-start = ((), (), s32[]{:S(2)}) async-start(), calls=%async_computation.9 | async-start | bytes 1310720 | tf_op jit(solution)/shard_map/reduce_scatter | solution.py:42
  19.3 114.6 %reduce-scatter.9.cloned.1.call-start = ((), (), s32[]{:S(2)}) async-start(), calls=%async_computation.6 | async-start | bytes 1310720 | tf_op jit(solution)/shard_map/reduce_scatter | solution.py:43
  23.3 206.1 %all-reduce.5.cloned.1.call-start = ((), (), s32[]{:S(2)}) async-start(), calls=%async_computation.10 | async-start | bytes 1048576 | tf_op jit(solution)/shard_map/psum | solution.py:84
  78.9 80.8 %copy-start.4 = (f32[32,8,128]{2,1,0:T(8,128)}, f32[32,8,128]{2,1,0:T(8,128)S(1)}, u32[]{:S(2)}) copy-start(f32[32,8,128]{2,1,0:T(8,128)S(1)} %multiply_add_fusion.1) | copy-start | bytes 393220
  159.7 36.1 %copy-start.3 = (bf16[2048,1024]{1,0:T(8,128)(2,1)S(1)}, bf16[2048,1024]{1,0:T(8,128)(2,1)}, u32[]{:S(2)}) copy-start(bf16[2048,1024]{1,0:T(8,128)(2,1)} %param.30) | copy-start | bytes 12582916
  159.7 37.8 %copy-start.8 = (bf16[1024]{0:T(1024)(128)(2,1)S(1)}, bf16[1024]{0:T(1024)(128)(2,1)}, u32[]{:S(2)}) copy-start(bf16[1024]{0:T(1024)(128)(2,1)} %param.31) | copy-start | bytes 6148
  197.5 83.0 %reduce-scatter.17.cloned.1.call-start = ((), (), s32[]{:S(2)}) async-start(), calls=%async_computation.11 | async-start | bytes 2621440 | tf_op jit(solution)/shard_map/reduce_scatter | solution.py:90
  236.5 73.3 %all-gather.2.cloned.1.call-start = ((), (), s32[]{:S(2)}) async-start(), calls=%async_computation.12 | async-start | bytes 1310720 | tf_op jit(solution)/shard_map/all_gather | solution.py:96
  282.4 66.7 %copy-start.1 = (bf16[1024,1024]{1,0:T(8,128)(2,1)S(1)}, bf16[1024,1024]{1,0:T(8,128)(2,1)}, u32[]{:S(2)}) copy-start(bf16[1024,1024]{1,0:T(8,128)(2,1)} %param.19) | copy-start | bytes 6291460
  282.4 65.0 %all-reduce.7.cloned.1.call-start = ((), (), s32[]{:S(2)}) async-start(), calls=%async_computation.13 | async-start | bytes 524288 | tf_op jit(solution)/shard_map/psum | solution.py:100
Sparse Core Ops, SparseCore 0:
  10.8 22.0 reduce-scatter.18
  35.2 19.9 reduce-scatter.10
  57.5 20.1 reduce-scatter.12
  80.3 25.5 reduce-scatter.14
  108.1 25.7 reduce-scatter.8
  197.6 31.7 all-reduce.4
  236.6 43.7 reduce-scatter.16
  282.6 27.1 all-gather.1
  315.6 31.6 all-reduce.6
where the time goes:
time: 356 us
  waiting for transfers between devices  216 us (61%)
  matrix products  47.9 us (13%)
  blocking collectives  41.2 us (12%)
  other arithmetic  34.2 us (10%)
  between operations  14.8 us (4%)
    psum x1, waiting for transfers between devices, per_device(): branch = lax.psum(branch, 'tp')  31.9 us
    reduce_scatter x1, waiting for transfers between devices, per_device(): lax.psum_scatter(up_part, 'kv', scatter_dimension=0, tiled=True)  31.8 us
    psum x1, waiting for transfers between devices, per_device(): down = lax.psum(down.astype(jnp.bfloat16), 'tp').astype(jnp.float32)  31.2 us
    reduce_scatter x1, waiting for transfers between devices, per_device(): lax.psum_scatter(product(outgate_weight), 'kv', scatter_dimension=0, tile...  27.9 us
    all_gather x1, waiting for transfers between devices, per_device(): lax.all_gather(hidden, 'kv', axis=0, tiled=True)  27.4 us
    reduce_scatter x1, waiting for transfers between devices, per_device(): lax.psum_scatter(product(value_weight), 'kv', scatter_dimension=0, tiled=...  26.9 us
    unnamed x2, blocking collectives  25.3 us
    add x1, other arithmetic, per_device(): fdecay[:, :, None, None] * state_matrix  24.5 us
  transfers between devices with their start and end apart: 9, of which 8 were waited for; matrix products, arithmetic and copies ran while one was open for 5% of the time, Pallas kernels for 0%

commit v1 on v0

--- a/solution.py
+++ b/solution.py
@@ -7,6 +7,11 @@
 DQK = 128
 DV = 256
 epsilon = 1e-06
+
+
+def gather_and_add(x, mesh_axis):
+    parts = lax.all_gather(x, mesh_axis)
+    return jnp.sum(parts, axis=0)
 
 
 def per_device(
@@ -97,7 +102,7 @@
         down_weight,
         preferred_element_type=jnp.float32,
     )
-    down = lax.psum(down.astype(jnp.bfloat16), "tp").astype(jnp.float32)
+    down = gather_and_add(down.astype(jnp.bfloat16), "tp").astype(jnp.float32)
     mixed_out = (resid + down).astype(jnp.bfloat16)
     return (mixed_out, new_matrix, new_norm, new_max)
 

time: 356 us -> 341 us (0.958)
  waiting for transfers between devices: 216 us -> 200 us
    psum x1 -> x0, waiting for transfers between devices: 31.2 us -> none  [per_device(): down = lax.psum(down.astype(jnp.bfloat16), 'tp').astype(jnp.float32)]
    all_gather x0 -> x1, waiting for transfers between devices: none -> 15.6 us  [gather_and_add(): parts = lax.all_gather(x, mesh_axis)]
where the time goes in v1:
time: 341 us; the launch traced here: 340 us
  waiting for transfers between devices  200 us (59%)
  matrix products  47.9 us (14%)
  blocking collectives  41.2 us (12%)
  other arithmetic  34.7 us (10%)
  between operations  14.8 us (4%)
    psum x1, waiting for transfers between devices, per_device(): branch = lax.psum(branch, 'tp')  31.9 us
    reduce_scatter x1, waiting for transfers between devices, per_device(): lax.psum_scatter(up_part, 'kv', scatter_dimension=0, tiled=True)  31.8 us
    reduce_scatter x1, waiting for transfers between devices, per_device(): lax.psum_scatter(product(outgate_weight), 'kv', scatter_dimension=0, tile...  27.9 us
    all_gather x1, waiting for transfers between devices, per_device(): lax.all_gather(hidden, 'kv', axis=0, tiled=True)  27.4 us
    reduce_scatter x1, waiting for transfers between devices, per_device(): lax.psum_scatter(product(value_weight), 'kv', scatter_dimension=0, tiled=...  26.9 us
    unnamed x2, blocking collectives  25.3 us
    add x1, other arithmetic, per_device(): fdecay[:, :, None, None] * state_matrix  24.5 us
    reduce_scatter x1, waiting for transfers between devices, per_device(): lax.psum_scatter(product(key_weight), 'kv', scatter_dimension=0, tiled=True)  22.4 us
  transfers between devices with their start and end apart: 9, of which 8 were waited for; matrix products, arithmetic and copies ran while one was open for 5% of the time, Pallas kernels for 0%

profile of v1, /device:TPU:0, one launch (start us, length us, event | category | flops | bytes accessed | tf_op | source)
XLA Modules:
  0.0 340.5 jit_solution(3619572743938683975)
XLA Ops:
  7.2 0.8 convert_element_type.63
  8.1 1.8 fusion.14
  10.0 2.2 fusion.16
  12.3 3.0 fusion.12
  15.3 4.0 %fusion.10 = f32[128,2048]{1,0:T(8,128)} fusion(bf16[1024,2048]{1,0:T(8,128)(2,1)} %param.21, bf16[128,1024]{1,0:T(8,128)(2,1)} %param.17, f32[1024]{0:T(1024)S(1)} %convert_element_type.63), kind=kOutput, calls=%fused_computation.30 | convolution fusion | flops 537264128 | bytes 5509120 | tf_op jit(solution)/shard_map/dot_general | solution.py:42
  19.4 3.9 %fusion.18 = f32[128,2048]{1,0:T(8,128)} fusion(bf16[1024,2048]{1,0:T(8,128)(2,1)} %param.22, bf16[128,1024]{1,0:T(8,128)(2,1)S(1)} %copy-done.2, f32[1024]{0:T(1024)S(1)} %convert_element_type.63), kind=kOutput, calls=%fused_computation.34 | convolution fusion | flops 537264128 | bytes 5509120 | tf_op jit(solution)/shard_map/dot_general | solution.py:42
  23.5 0.6 dynamic-slice
  24.9 13.4 %all-reduce = f32[128]{0:T(128)S(1)} all-reduce(f32[128]{0:T(128)S(1)} %fusion.1), channel_id=4, replica_groups=mesh['grp'=2,'kv'=4,'tp'=4] {'kv'}, use_global_device_ids=true, to_apply=%region_2.0.clone | all-reduce | flops 128 | bytes 1024
  38.4 0.8 broadcast_multiply_fusion
  39.3 15.9 %reduce-scatter.11.cloned.1.call-done = f32[32,1024]{1,0:T(8,128)} async-done(((f32[128,1024]{1,0:T(8,128)}), f32[32,1024]{1,0:T(8,128)}) %reduce-scatter.11.cloned.1.call-update) | async-done | bytes 131088 | tf_op jit(solution)/shard_map/reduce_scatter | solution.py:45
  55.2 22.4 %reduce-scatter.13.cloned.1.call-done = f32[32,1024]{1,0:T(8,128)} async-done(((f32[128,1024]{1,0:T(8,128)}), f32[32,1024]{1,0:T(8,128)}) %reduce-scatter.13.cloned.1.call-update) | async-done | bytes 131088 | tf_op jit(solution)/shard_map/reduce_scatter | solution.py:46
  77.6 1.1 multiply_convert_fusion.3
  79.1 26.9 %reduce-scatter.15.cloned.1.call-done = f32[32,2048]{1,0:T(8,128)} async-done(((f32[128,2048]{1,0:T(8,128)}), f32[32,2048]{1,0:T(8,128)}) %reduce-scatter.15.cloned.1.call-update) | async-done | bytes 262160 | tf_op jit(solution)/shard_map/reduce_scatter | solution.py:47
  105.9 27.9 %reduce-scatter.9.cloned.1.call-done = f32[32,2048]{1,0:T(8,128)} async-done(((f32[128,2048]{1,0:T(8,128)}), f32[32,2048]{1,0:T(8,128)}) %reduce-scatter.9.cloned.1.call-update) | async-done | bytes 262160 | tf_op jit(solution)/shard_map/reduce_scatter | solution.py:48
  133.9 1.1 multiply_convert_fusion.1
  135.2 24.5 %multiply_add_fusion = f32[32,8,128,256]{3,2,1,0:T(8,128)} fusion(f32[32,8,128,256]{3,2,1,0:T(8,128)} %param.26, f32[32,8,256]{2,1,0:T(8,128)S(1)} %bitcast.46, f32[32,8,128]{2,1,0:T(8,128)S(1)} %bitcast.45, f32[32,8]{1,0:T(8,128)S(1)} %subtract_exponential_fusion, f32[32,8]{1,0:T(8,128)S(1)} %get-tuple-element.8), kind=kLoop, calls=%fused_computation | loop fusion | flops 33554432 | bytes 67504128 | tf_op jit(solution)/shard_map/add | solution.py:72
  159.8 19.8 %fusion.31 = f32[32,8,1,256]{3,2,1,0:T(1,128)S(1)} fusion(f32[32,8,128,1]{2,3,1,0:T(1,128)S(1)} %bitcast.44, f32[32,8,128,256]{3,2,1,0:T(8,128)} %multiply_add_fusion), kind=kOutput, calls=%fused_computation.56 | convolution fusion | flops 100663296 | bytes 33947648 | tf_op jit(solution)/shard_map/bhd,bhde->bhe/dot_general | solution.py:76
  179.6 0.2 multiply_reduce_fusion
  179.9 16.0 %all_gather.12 = bf16[128,2048]{1,0:T(8,128)(2,1)S(1)} all-gather(bf16[32,2048]{1,0:T(8,128)(2,1)S(1)} %bitcast.49), channel_id=1, replica_groups=mesh['grp'=2,'kv'=4,'tp'=4] {'kv'}, dimensions={0}, use_global_device_ids=true | all-gather | bytes 655360 | tf_op jit(solution)/shard_map/all_gather | solution.py:85
  195.9 1.6 fusion.32
  197.5 31.9 %all-reduce.4.cloned.1.call-done = f32[128,1024]{1,0:T(8,128)} async-done(((f32[128,1024]{1,0:T(8,128)}), f32[128,1024]{1,0:T(8,128)}) %all-reduce.4.cloned.1.call-update) | async-done | bytes 524304 | tf_op jit(solution)/shard_map/psum | solution.py:89
  229.4 1.1 fusion.2
  230.5 6.0 %fusion.6 = f32[128,4096]{1,0:T(8,128)} fusion(bf16[1024,4096]{1,0:T(8,128)(2,1)} %param.32, bf16[128,1024]{1,0:T(8,128)(2,1)S(1)} %fusion.2, f32[1024]{0:T(1024)S(1)} %convert_element_type.75), kind=kOutput, calls=%fused_computation.15 | convolution fusion | flops 1074135040 | bytes 10752000 | tf_op jit(solution)/shard_map/dot_general | solution.py:93
  236.7 11.8 %all-reduce.1 = f32[128]{0:T(128)S(1)} all-reduce(f32[128]{0:T(128)S(1)} %fusion.4), channel_id=10, replica_groups=mesh['grp'=2,'kv'=4,'tp'=4] {'kv'}, use_global_device_ids=true, to_apply=%region_12.13.clone | all-reduce | flops 128 | bytes 1024
  248.6 31.8 %reduce-scatter.17.cloned.1.call-done = f32[32,4096]{1,0:T(8,128)} async-done(((f32[128,4096]{1,0:T(8,128)}), f32[32,4096]{1,0:T(8,128)}) %reduce-scatter.17.cloned.1.call-update) | async-done | bytes 524304 | tf_op jit(solution)/shard_map/reduce_scatter | solution.py:95
  280.5 1.9 multiply_convert_fusion
  282.4 27.4 %all-gather.4.cloned.1.call-done = bf16[128,4096]{1,0:T(8,128)(2,1)} async-done(((bf16[32,4096]{1,0:T(8,128)(2,1)}), bf16[128,4096]{1,0:T(8,128)(2,1)}) %all-gather.4.cloned.1.call-update) | async-done | bytes 1048592 | tf_op jit(solution)/shard_map/all_gather | solution.py:101
  309.8 5.7 %convolution_convert_fusion = bf16[128,1024]{1,0:T(8,128)(2,1)} fusion(bf16[128,4096]{1,0:T(8,128)(2,1)} %all-gather.4.cloned.1.call-done, bf16[4096,1024]{1,0:T(8,128)(2,1)} %param.33), kind=kOutput, calls=%fused_computation.1 | convolution fusion | flops 1073872896 | bytes 9699328 | tf_op jit(solution)/shard_map/dot_general | solution.py:100
  315.5 0.7 copy.28
  316.2 15.6 %all-gather.6.cloned.1.call-done = bf16[512,1024]{1,0:T(8,128)(2,1)} async-done(((bf16[128,1024]{1,0:T(8,128)(2,1)}), bf16[512,1024]{1,0:T(8,128)(2,1)}) %all-gather.6.cloned.1.call-update) | async-done | bytes 1048592 | tf_op jit(solution)/shard_map/all_gather | solution.py:13
  331.8 1.4 reduce_sum.52
  333.2 0.8 fusion.5
  (63 shorter events, 1.9 us)
Async XLA Ops:
  7.2 2.8 copy-start
  7.2 12.2 %copy-start.2 = (bf16[128,1024]{1,0:T(8,128)(2,1)S(1)}, bf16[128,1024]{1,0:T(8,128)(2,1)}, u32[]{:S(2)}) copy-start(bf16[128,1024]{1,0:T(8,128)(2,1)} %param.17) | copy-start | bytes 786436
  7.2 31.2 %reduce-scatter.19.cloned.1.call-start = ((), (), s32[]{:S(2)}) async-start(), calls=%async_computation.14 | async-start | bytes 81920 | tf_op jit(solution)/shard_map/reduce_scatter | solution.py:49
  9.9 45.3 %reduce-scatter.11.cloned.1.call-start = ((), (), s32[]{:S(2)}) async-start(), calls=%async_computation.7 | async-start | bytes 655360 | tf_op jit(solution)/shard_map/reduce_scatter | solution.py:45
  12.2 11.3 %copy-start.10 = (u32[32]{0:T(128)S(1)}, u32[32]{0:T(128)}, u32[]{:S(2)}) copy-start(u32[32]{0:T(128)} %constant.25) | copy-start | bytes 388
  12.2 12.5 %copy-start.6 = (bf16[2048]{0:T(1024)(128)(2,1)S(1)}, bf16[2048]{0:T(1024)(128)(2,1)}, u32[]{:S(2)}) copy-start(bf16[2048]{0:T(1024)(128)(2,1)} %param.29) | copy-start | bytes 12292
  12.2 12.6 %copy-start.7 = (f32[32,8]{0,1:T(8,128)S(1)}, f32[32,8]{0,1:T(8,128)}, u32[]{:S(2)}) copy-start(f32[32,8]{0,1:T(8,128)} %param.28) | copy-start | bytes 3076
  12.2 26.9 %copy-start.9 = (f32[8]{0:T(128)S(1)}, f32[8]{0:T(128)}, u32[]{:S(2)}) copy-start(f32[8]{0:T(128)} %param.25) | copy-start | bytes 100
  12.3 65.4 %reduce-scatter.13.cloned.1.call-start = ((), (), s32[]{:S(2)}) async-start(), calls=%async_computation.8 | async-start | bytes 655360 | tf_op jit(solution)/shard_map/reduce_scatter | solution.py:46
  15.3 63.5 %copy-start.5 = (f32[32,8,128]{2,1,0:T(8,128)S(1)}, f32[32,8,128]{2,1,0:T(8,128)}, u32[]{:S(2)}) copy-start(f32[32,8,128]{2,1,0:T(8,128)} %param.27) | copy-start | bytes 393220
  15.3 90.7 %reduce-scatter.15.cloned.1.call-start = ((), (), s32[]{:S(2)}) async-start(), calls=%async_computation.9 | async-start | bytes 1310720 | tf_op jit(solution)/shard_map/reduce_scatter | solution.py:47
  19.3 114.6 %reduce-scatter.9.cloned.1.call-start = ((), (), s32[]{:S(2)}) async-start(), calls=%async_computation.6 | async-start | bytes 1310720 | tf_op jit(solution)/shard_map/reduce_scatter | solution.py:48
  23.3 206.1 %all-reduce.4.cloned.1.call-start = ((), (), s32[]{:S(2)}) async-start(), calls=%async_computation.10 | async-start | bytes 1048576 | tf_op jit(solution)/shard_map/psum | solution.py:89
  78.9 80.8 %copy-start.4 = (f32[32,8,128]{2,1,0:T(8,128)}, f32[32,8,128]{2,1,0:T(8,128)S(1)}, u32[]{:S(2)}) copy-start(f32[32,8,128]{2,1,0:T(8,128)S(1)} %multiply_add_fusion.1) | copy-start | bytes 393220
  159.7 36.1 %copy-start.3 = (bf16[2048,1024]{1,0:T(8,128)(2,1)S(1)}, bf16[2048,1024]{1,0:T(8,128)(2,1)}, u32[]{:S(2)}) copy-start(bf16[2048,1024]{1,0:T(8,128)(2,1)} %param.30) | copy-start | bytes 12582916
  159.7 37.8 %copy-start.8 = (bf16[1024]{0:T(1024)(128)(2,1)S(1)}, bf16[1024]{0:T(1024)(128)(2,1)}, u32[]{:S(2)}) copy-start(bf16[1024]{0:T(1024)(128)(2,1)} %param.31) | copy-start | bytes 6148
  197.5 83.0 %reduce-scatter.17.cloned.1.call-start = ((), (), s32[]{:S(2)}) async-start(), calls=%async_computation.11 | async-start | bytes 2621440 | tf_op jit(solution)/shard_map/reduce_scatter | solution.py:95
  236.5 73.3 %all-gather.4.cloned.1.call-start = ((), (), s32[]{:S(2)}) async-start(), calls=%async_computation.12 | async-start | bytes 1310720 | tf_op jit(solution)/shard_map/all_gather | solution.py:101
  282.4 51.6 %copy-start.1 = (bf16[1024,1024]{1,0:T(8,128)(2,1)S(1)}, bf16[1024,1024]{1,0:T(8,128)(2,1)}, u32[]{:S(2)}) copy-start(bf16[1024,1024]{1,0:T(8,128)(2,1)} %param.19) | copy-start | bytes 6291460
  282.4 49.4 %all-gather.6.cloned.1.call-start = ((), (), s32[]{:S(2)}) async-start(), calls=%async_computation.13 | async-start | bytes 1310720 | tf_op jit(solution)/shard_map/all_gather | solution.py:13
Sparse Core Ops, SparseCore 0:
  10.8 22.0 reduce-scatter.18
  35.2 19.9 reduce-scatter.10
  57.5 20.1 reduce-scatter.12
  80.3 25.5 reduce-scatter.14
  108.1 25.7 reduce-scatter.8
  197.6 31.7 all-reduce.3
  236.6 43.7 reduce-scatter.16
  282.6 27.1 all-gather.3
  315.6 16.0 all-gather.5
